TPU v7x, 32 devices: a whole 2x2x4 slice. The times are simulated.
32 devices in a mesh: sp: 8 (over z, x), tp: 4 (over y, core).
Axes of the slice: x: 2, y: 2, z: 4, core: 2. Of those that a mesh axis runs over, the one named last changes fastest.
Arguments:
- residual: bfloat16 [2048, 2048], P(('sp', 'tp')), may hold values from -6 to 6
- first_query: bfloat16 [2048, 512], P('sp', 'tp'), may hold values from -6 to 6
- second_query: bfloat16 [2048, 512], P('sp', 'tp'), may hold values from -6 to 6
- first_key: bfloat16 [2048, 512], P('sp', 'tp'), may hold values from -6 to 6
- second_key: bfloat16 [2048, 512], P('sp', 'tp'), may hold values from -6 to 6
- values: bfloat16 [2048, 1024], P('sp', 'tp'), may hold values from -6 to 6
- lambdas: float32 [8], P('tp'), may hold values from 0.3 to 0.8
- head_gain: float32 [128], replicated, may hold values from 0.1 to 1.9
- out_weight: bfloat16 [1024, 2048], P('tp'), may hold values from -0.1875 to 0.1875
- norm_gain: float32 [2048], replicated, may hold values from 0.1 to 1.9
- up_weight: bfloat16 [2048, 4096], P('sp', 'tp'), may hold values from -0.125 to 0.125
- down_weight: bfloat16 [4096, 2048], P('tp', 'sp'), may hold values from -0.09375 to 0.09375
Outputs:
- mixed: bfloat16 [2048, 2048], P(('sp', 'tp'))
All inputs are finite; a program needn't handle non-finite values.
Results may differ from a plain program's by a relative error of at most 0.019.
Values may be sent and summed in bfloat16 or wider, within the bound.
A program may use at most 128 MiB of HBM per device.

v0:
```python
import jax
import jax.numpy as jnp
from jax import lax
from jax.sharding import PartitionSpec as P


def rotate(blocked, positions):
    half = blocked.shape[-1] // 2
    inverse = 10000.0 ** (-jnp.arange(0, half, dtype=jnp.float32) * 2.0 / blocked.shape[-1])
    angle = positions[:, None] * inverse[None, :]
    cosine = jnp.cos(angle)[:, None, :]
    sine = jnp.sin(angle)[:, None, :]
    first, second = (blocked[..., :half], blocked[..., half:])
    return jnp.concatenate(
        [first * cosine - second * sine, second * cosine + first * sine], axis=-1
    )


def absorb(state, queries, keys, vals, factor):
    top, total, summed = state
    scores = jnp.einsum("qhe,khe->qhk", queries, keys, preferred_element_type=jnp.float32) * factor
    peak = jnp.maximum(top, jnp.max(scores, axis=-1))
    shrink = jnp.exp(top - peak)
    weights = jnp.exp(scores - peak[..., None])
    total = total * shrink + jnp.sum(weights, axis=-1)
    summed = summed * shrink[..., None] + jnp.einsum(
        "qhk,khe->qhe", weights.astype(jnp.bfloat16), vals, preferred_element_type=jnp.float32
    )
    return (peak, total, summed)


def layer_norm(stream, gain):
    center = stream - jnp.mean(stream, axis=-1, keepdims=True)
    spread = jnp.mean(center * center, axis=-1, keepdims=True)
    return center * lax.rsqrt(spread + 1e-05) * gain


def local(
    residual,
    first_query,
    second_query,
    first_key,
    second_key,
    values,
    lambdas,
    head_gain,
    out_weight,
    norm_gain,
    up_weight,
    down_weight,
):
    local_rows = first_query.shape[0]
    head_count = lambdas.shape[0]
    head_width = first_query.shape[1] // head_count
    value_width = values.shape[1] // head_count
    quarter_rows = local_rows // lax.axis_size("tp")
    factor = head_width ** (-0.5)
    positions = (lax.axis_index("sp") * local_rows + jnp.arange(local_rows)).astype(jnp.float32)

    def prepare(source):
        turned = rotate(
            source.astype(jnp.float32).reshape(local_rows, head_count, head_width), positions
        )
        return turned.astype(jnp.bfloat16)

    query_a, query_b = (prepare(first_query), prepare(second_query))
    key_a = prepare(first_key).reshape(local_rows, head_count * head_width)
    key_b = prepare(second_key).reshape(local_rows, head_count * head_width)
    start_state = (
        jnp.full((local_rows, head_count), -1e30, jnp.float32),
        jnp.zeros((local_rows, head_count), jnp.float32),
        jnp.zeros((local_rows, head_count, value_width), jnp.float32),
    )
    piece_a = lax.all_gather(key_a, "sp", axis=0, tiled=True)
    piece_b = lax.all_gather(key_b, "sp", axis=0, tiled=True)
    piece_v = lax.all_gather(values, "sp", axis=0, tiled=True)
    count = piece_a.shape[0]
    block = 512
    blocks = count // block

    def advance(state, item):
        block_a, block_b, block_v = item
        return (
            (
                absorb(state[0], query_a, block_a, block_v, factor),
                absorb(state[1], query_b, block_b, block_v, factor),
            ),
            None,
        )

    items = (
        piece_a.reshape(blocks, block, head_count, head_width),
        piece_b.reshape(blocks, block, head_count, head_width),
        piece_v.reshape(blocks, block, head_count, value_width),
    )
    state_a, state_b = lax.scan(advance, (start_state, start_state), items)[0]
    diff = state_a[2] / state_a[1][..., None] - lambdas[None, :, None] * (
        state_b[2] / state_b[1][..., None]
    )
    scale = lax.rsqrt(jnp.mean(diff * diff, axis=-1, keepdims=True) + 1e-05)
    flat = (
        (diff * scale * head_gain * 0.8)
        .astype(jnp.bfloat16)
        .reshape(local_rows, head_count * value_width)
    )
    projected = lax.psum(
        jnp.dot(flat, out_weight, preferred_element_type=jnp.float32).astype(jnp.bfloat16), "tp"
    ).astype(jnp.float32)
    stream = lax.all_gather(residual, "tp", axis=0, tiled=True)
    whole = layer_norm(stream.astype(jnp.float32) + projected, norm_gain).astype(jnp.bfloat16)
    own_normed = lax.dynamic_slice_in_dim(
        whole, lax.axis_index("tp") * quarter_rows, quarter_rows, 0
    )
    lifted = jnp.dot(
        whole,
        lax.all_gather(up_weight, "sp", axis=0, tiled=True),
        preferred_element_type=jnp.float32,
    )
    down_full = lax.all_gather(down_weight, "sp", axis=1, tiled=True)
    hidden = jnp.square(jax.nn.relu(lifted)).astype(jnp.bfloat16)
    lowered = lax.psum_scatter(
        jnp.dot(hidden, down_full, preferred_element_type=jnp.float32).astype(jnp.bfloat16),
        "tp",
        scatter_dimension=0,
        tiled=True,
    ).astype(jnp.float32)
    return (own_normed.astype(jnp.float32) + lowered).astype(jnp.bfloat16)


def solution(mesh):
    in_specs = (
        P(("sp", "tp"), None),
        P("sp", "tp"),
        P("sp", "tp"),
        P("sp", "tp"),
        P("sp", "tp"),
        P("sp", "tp"),
        P("tp"),
        P(),
        P("tp", None),
        P(),
        P("sp", "tp"),
        P("tp", "sp"),
    )
    out_specs = P(("sp", "tp"), None)
    return jax.shard_map(local, mesh=mesh, in_specs=in_specs, out_specs=out_specs, check_vma=False)
```

profile of v0, /device:TPU:0, one launch (start us, length us, event | category | flops | bytes accessed | tf_op | source)
XLA Modules:
  0.0 354.3 jit_solution(2607594345238030326)
XLA Ops:
  6.5 0.7 all-gather.7.cloned.1.call-update
  8.1 0.9 copy.21
  9.1 0.9 copy.22
  10.0 0.9 copy.23
  11.0 0.9 copy.24
  12.2 34.2 %all_gather.21 = bf16[2048,128]{0,1:T(8,128)(2,1)S(1)} all-gather(bf16[256,128]{0,1:T(8,128)(2,1)S(1)} %bitcast.66), channel_id=1, replica_groups=mesh['sp'=8,'tp'=4] {'sp'}, dimensions={0}, use_global_device_ids=true | all-gather | bytes 589824 | tf_op jit(solution)/shard_map/all_gather | solution.py:75
  46.8 0.9 copy.27
  47.7 31.6 %all_gather.19 = bf16[2048,128]{0,1:T(8,128)(2,1)S(1)} all-gather(bf16[256,128]{0,1:T(8,128)(2,1)S(1)} %bitcast.67), channel_id=1, replica_groups=mesh['sp'=8,'tp'=4] {'sp'}, dimensions={0}, use_global_device_ids=true | all-gather | bytes 589824 | tf_op jit(solution)/shard_map/all_gather | solution.py:74
  79.7 0.9 copy.25
  80.6 2.1 reshape.134
  82.7 42.6 %while.21 = (s32[]{:T(128)}, f32[256,2]{0,1:T(2,128)S(1)}, f32[256,2]{0,1:T(2,128)}, f32[256,2,128]{0,2,1:T(8,128)}, f32[256,2]{0,1:T(2,128)S(1)}, /*index=5*/f3...) while((s32[]{:T(128)}, f32[256,2]{0,1:T(2,128)S(1)}, ...), condition=%wide.region_5.6_spmd.clone, body=%wide.region_0.5_spmd.clone.sunk | while | flops 204870656 | bytes 9381043 | solution.py:96
  82.7 1.3 fusion.60
  84.2 1.3 fusion.62
  86.3 1.8 constant_dynamic-slice_fusion.2
  88.1 1.1 copy.32
  89.2 1.7 fusion.68
  90.9 1.0 fusion.67
  92.0 1.3 fusion.60
  93.4 1.3 fusion.62
  94.9 1.3 fusion.66
  96.2 1.8 constant_dynamic-slice_fusion.2
  98.0 1.1 copy.32
  99.1 2.0 fusion.68
  101.1 2.0 fusion.67
  103.1 1.3 fusion.60
  104.5 1.3 fusion.62
  106.0 1.3 fusion.66
  107.3 1.8 constant_dynamic-slice_fusion.2
  109.1 1.1 copy.32
  110.2 2.0 fusion.68
  112.2 2.0 fusion.67
  114.2 1.3 fusion.60
  115.7 1.3 fusion.62
  117.1 1.3 fusion.66
  118.4 1.8 constant_dynamic-slice_fusion.2
  120.3 1.1 copy.32
  121.4 2.0 fusion.68
  123.4 2.0 fusion.67
  125.3 1.2 multiply_reduce_fusion.1
  126.5 0.7 multiply_convert_fusion.1
  127.3 1.4 convolution_convert_fusion.1
  130.0 35.5 %all-reduce.2.cloned.1.call-done = bf16[256,2048]{1,0:T(8,128)(2,1)} async-done(((bf16[256,2048]{1,0:T(8,128)(2,1)}), bf16[256,2048]{1,0:T(8,128)(2,1)}) %all-reduce.2.cloned.1.call-update) | async-done | bytes 1048592 | tf_op jit(solution)/shard_map/psum | solution.py:106
  165.4 2.0 fusion.25
  168.5 74.0 %all-gather.11.cloned.1.call-done = bf16[1024,2048]{1,0:T(8,128)(2,1)} async-done(((bf16[1024,256]{1,0:T(8,128)(2,1)}), bf16[1024,2048]{1,0:T(8,128)(2,1)}) %all-gather.11.cloned.1.call-update) | async-done | bytes 4194320 | tf_op jit(solution)/shard_map/all_gather | solution.py:119
  242.5 73.0 %all-gather.9.cloned.1.call-done = bf16[2048,1024]{1,0:T(8,128)(2,1)} async-done(((bf16[256,1024]{1,0:T(8,128)(2,1)}), bf16[2048,1024]{1,0:T(8,128)(2,1)}) %all-gather.9.cloned.1.call-update) | async-done | bytes 4194320 | tf_op jit(solution)/shard_map/all_gather | solution.py:116
  315.5 6.8 %convolution_convert_fusion = bf16[256,2048]{1,0:T(8,128)(2,1)} fusion(bf16[1024,2048]{1,0:T(8,128)(2,1)} %all-gather.11.cloned.1.call-done, bf16[256,2048]{1,0:T(8,128)(2,1)S(1)} %multiply_convert_fusion, bf16[2048,1024]{1,0:T(8,128)(2,1)} %all-gather.9.cloned.1.call-done), kind=kOutput, calls=%fused_computation.37 | convolution fusion | flops 2148794368 | bytes 10485760 | tf_op jit(solution)/shard_map/dot_general | solution.py:122
  322.3 23.5 %reduce-scatter.2.cloned.1.call-done = bf16[64,2048]{1,0:T(8,128)(2,1)} async-done(((bf16[256,2048]{1,0:T(8,128)(2,1)}), bf16[64,2048]{1,0:T(8,128)(2,1)}) %reduce-scatter.2.cloned.1.call-update) | async-done | bytes 262160 | tf_op jit(solution)/shard_map/reduce_scatter | solution.py:121
  345.8 1.7 add_convert_fusion
  (74 shorter events, 6.1 us)
Async XLA Ops:
  6.5 120.7 %copy-start = (bf16[256,2048]{1,0:T(8,128)(2,1)S(1)}, bf16[256,2048]{1,0:T(8,128)(2,1)}, u32[]{:S(2)}) copy-start(bf16[256,2048]{1,0:T(8,128)(2,1)} %param.22) | copy-start | bytes 3145732
  6.5 74.1 %all-gather.7.cloned.1.call-start = ((), (), s32[]{:S(2)}) async-start(), calls=%async_computation.2 | async-start | bytes 1179648 | tf_op jit(solution)/shard_map/all_gather | solution.py:76
  7.3 122.7 %all-gather.5.cloned.1.call-start = ((), (), s32[]{:S(2)}) async-start(), calls=%async_computation.1 | async-start | bytes 1310720 | tf_op jit(solution)/shard_map/all_gather | solution.py:109
  8.0 157.4 %all-reduce.2.cloned.1.call-start = ((), (), s32[]{:S(2)}) async-start(), calls=%async_computation.3 | async-start | bytes 2097152 | tf_op jit(solution)/shard_map/psum | solution.py:106
  86.3 4.7 %copy-start.3 = (f32[256,2]{0,1:T(2,128)S(1)}, f32[256,2]{0,1:T(2,128)}, u32[]{:S(2)}) copy-start(f32[256,2]{0,1:T(2,128)} %get-tuple-element.265) | copy-start | bytes 6148 | tf_op jit(solution)/shard_map/while
  96.2 4.9 %copy-start.3 = (f32[256,2]{0,1:T(2,128)S(1)}, f32[256,2]{0,1:T(2,128)}, u32[]{:S(2)}) copy-start(f32[256,2]{0,1:T(2,128)} %get-tuple-element.265) | copy-start | bytes 6148 | tf_op jit(solution)/shard_map/while
  107.3 4.9 %copy-start.3 = (f32[256,2]{0,1:T(2,128)S(1)}, f32[256,2]{0,1:T(2,128)}, u32[]{:S(2)}) copy-start(f32[256,2]{0,1:T(2,128)} %get-tuple-element.265) | copy-start | bytes 6148 | tf_op jit(solution)/shard_map/while
  118.4 4.9 %copy-start.3 = (f32[256,2]{0,1:T(2,128)S(1)}, f32[256,2]{0,1:T(2,128)}, u32[]{:S(2)}) copy-start(f32[256,2]{0,1:T(2,128)} %get-tuple-element.265) | copy-start | bytes 6148 | tf_op jit(solution)/shard_map/while
  128.7 113.7 %all-gather.11.cloned.1.call-start = ((), (), s32[]{:S(2)}) async-start(), calls=%async_computation.5 | async-start | bytes 4718592 | tf_op jit(solution)/shard_map/all_gather | solution.py:119
  129.3 186.1 %all-gather.9.cloned.1.call-start = ((), (), s32[]{:S(2)}) async-start(), calls=%async_computation.4 | async-start | bytes 4718592 | tf_op jit(solution)/shard_map/all_gather | solution.py:116
  129.4 38.6 %copy-start.4 = (f32[2048]{0:T(1024)S(1)}, f32[2048]{0:T(1024)}, u32[]{:S(2)}) copy-start(f32[2048]{0:T(1024)} %param.23) | copy-start | bytes 24580
  129.9 215.9 %reduce-scatter.2.cloned.1.call-start = ((), (), s32[]{:S(2)}) async-start(), calls=%async_computation.6 | async-start | bytes 1310720 | tf_op jit(solution)/shard_map/reduce_scatter | solution.py:121
  130.0 37.5 %copy-start.1 = (bf16[256,2048]{1,0:T(8,128)(2,1)S(1)}, bf16[256,2048]{1,0:T(8,128)(2,1)}, u32[]{:S(2)}) copy-start(bf16[256,2048]{1,0:T(8,128)(2,1)} %all-gather.5.cloned.1.call-done) | copy-start | bytes 3145732
  165.4 2.0 copy-start.2
Sparse Core Ops, SparseCore 0:
  9.5 45.4 all-gather.6
  56.5 15.4 all-gather.4
  128.9 36.5 all-reduce.1
  167.3 75.0 all-gather.10
  244.4 70.9 all-gather.8
  322.4 23.2 reduce-scatter.1
where the time goes:
time: 355 us; the launch traced here: 354 us
  waiting for transfers between devices  208 us (59%)
  blocking collectives  65.8 us (19%)
  matrix products  33 us (9%)
  local copies, waits for them, and re-layouts  20.2 us (6%)
  between operations  13.7 us (4%)
  other arithmetic  12.9 us (4%)
    all_gather x1, waiting for transfers between devices, local(): down_full = lax.all_gather(down_weight, 'sp', axis=1, tiled=True)  74 us
    all_gather x1, waiting for transfers between devices, local(): lax.all_gather(up_weight, 'sp', axis=0, tiled=True)  73 us
    psum x1, waiting for transfers between devices, local(): lax.psum(jnp.dot(flat, out_weight, preferred_element_type=jnp.float32).as...  35.5 us
    all_gather x1, blocking collectives, local(): piece_b = lax.all_gather(key_b, 'sp', axis=0, tiled=True)  34.2 us
    all_gather x1, blocking collectives, local(): piece_a = lax.all_gather(key_a, 'sp', axis=0, tiled=True)  31.6 us
    reduce_scatter x1, waiting for transfers between devices, local(): lax.psum_scatter(jnp.dot(hidden, down_full, preferred_element_type=jnp.fl...  23.5 us
    dot_general x8, matrix products, absorb(): jnp.einsum('qhk,khe->qhe', weights.astype(jnp.bfloat16), vals, preferred_...  14.6 us
    dynamic_slice x8, local copies, waits for them, and re-layouts, local(): state_a, state_b = lax.scan(advance, (start_state, start_state), items)[0]  11.8 us
  transfers between devices with their start and end apart: 6, of which 4 were waited for; matrix products, arithmetic and copies ran while one was open for 16% of the time, Pallas kernels for 0%

commit v1 on v0

--- a/solution.py
+++ b/solution.py
@@ -116,7 +116,9 @@
         lax.all_gather(up_weight, "sp", axis=0, tiled=True),
         preferred_element_type=jnp.float32,
     )
-    down_full = lax.all_gather(down_weight, "sp", axis=1, tiled=True)
+    down_full = jnp.concatenate(
+        lax.all_to_all(jnp.stack([down_weight] * lax.axis_size("sp")), "sp", 0, 0), axis=1
+    )
     hidden = jnp.square(jax.nn.relu(lifted)).astype(jnp.bfloat16)
     lowered = lax.psum_scatter(
         jnp.dot(hidden, down_full, preferred_element_type=jnp.float32).astype(jnp.bfloat16),

time: 355 us -> 309 us (0.87)
  waiting for transfers between devices: 208 us -> 155 us
  starting transfers between devices: 0.2 us -> 5.04 us
    all_to_all x0 -> x1, waiting for transfers between devices: none -> 97.4 us  [local(): lax.all_to_all(jnp.stack([down_weight] * lax.axis_size('sp')), 'sp', 0, 0)]
    all_gather x1 -> x0, waiting for transfers between devices: 74 us -> none  [local(): down_full = lax.all_gather(down_weight, 'sp', axis=1, tiled=True)]
    all_gather x1, waiting for transfers between devices: 73 us -> 3.25 us  [local(): lax.all_gather(up_weight, 'sp', axis=0, tiled=True)]
    psum x1, waiting for transfers between devices: 35.5 us -> 28.8 us  [local(): lax.psum(jnp.dot(flat, out_weight, preferred_element_type=jnp.float32).as...]
    all_to_all x0 -> x1, starting transfers between devices: none -> 4.89 us  [local(): lax.all_to_all(jnp.stack([down_weight] * lax.axis_size('sp')), 'sp', 0, 0)]
  transfers between devices with their start and end apart: 6 -> 6, of which waited for: 4 -> 4; matrix products, arithmetic and copies ran while one was open for 16% -> 20% of each run, Pallas kernels for 0% -> 0%
where the time goes in v1:
time: 309 us; the launch traced here: 308 us
  waiting for transfers between devices  155 us (50%)
  blocking collectives  65.8 us (21%)
  matrix products  33 us (11%)
  local copies, waits for them, and re-layouts  22.9 us (7%)
  between operations  13.4 us (4%)
  other arithmetic  12.9 us (4%)
  starting transfers between devices  5.04 us (2%)
    all_to_all x1, waiting for transfers between devices, local(): lax.all_to_all(jnp.stack([down_weight] * lax.axis_size('sp')), 'sp', 0, 0)  97.4 us
    all_gather x1, blocking collectives, local(): piece_a = lax.all_gather(key_a, 'sp', axis=0, tiled=True)  34.2 us
    all_gather x1, blocking collectives, local(): piece_b = lax.all_gather(key_b, 'sp', axis=0, tiled=True)  31.6 us
    psum x1, waiting for transfers between devices, local(): lax.psum(jnp.dot(flat, out_weight, preferred_element_type=jnp.float32).as...  28.8 us
    reduce_scatter x1, waiting for transfers between devices, local(): lax.psum_scatter(jnp.dot(hidden, down_full, preferred_element_type=jnp.fl...  23.7 us
    dot_general x8, matrix products, absorb(): jnp.einsum('qhk,khe->qhe', weights.astype(jnp.bfloat16), vals, preferred_...  14.6 us
    dynamic_slice x8, local copies, waits for them, and re-layouts, local(): state_a, state_b = lax.scan(advance, (start_state, start_state), items)[0]  11.8 us
    dot_general x8, matrix products, absorb(): jnp.einsum('qhe,khe->qhk', queries, keys, preferred_element_type=jnp.floa...  10.1 us
  transfers between devices with their start and end apart: 6, of which 4 were waited for; matrix products, arithmetic and copies ran while one was open for 20% of the time, Pallas kernels for 0%

profile of v1, /device:TPU:0, one launch (start us, length us, event | category | flops | bytes accessed | tf_op | source)
XLA Modules:
  0.0 308.4 jit_solution(15751025213946851446)
XLA Ops:
  8.1 0.9 copy.21
  9.1 0.9 copy.22
  10.0 0.9 copy.23
  11.0 0.9 copy.24
  12.2 34.2 %all_gather.16 = bf16[2048,128]{0,1:T(8,128)(2,1)S(1)} all-gather(bf16[256,128]{0,1:T(8,128)(2,1)S(1)} %bitcast.69), channel_id=1, replica_groups=mesh['sp'=8,'tp'=4] {'sp'}, dimensions={0}, use_global_device_ids=true | all-gather | bytes 589824 | tf_op jit(solution)/shard_map/all_gather | solution.py:74
  46.8 0.9 copy.25
  47.7 31.6 %all_gather.18 = bf16[2048,128]{0,1:T(8,128)(2,1)S(1)} all-gather(bf16[256,128]{0,1:T(8,128)(2,1)S(1)} %bitcast.70), channel_id=1, replica_groups=mesh['sp'=8,'tp'=4] {'sp'}, dimensions={0}, use_global_device_ids=true | all-gather | bytes 589824 | tf_op jit(solution)/shard_map/all_gather | solution.py:75
  79.7 0.9 copy.27
  80.6 2.1 reshape.142
  82.7 42.6 %while.21 = (s32[]{:T(128)}, f32[256,2]{0,1:T(2,128)S(1)}, f32[256,2]{0,1:T(2,128)}, f32[256,2,128]{0,2,1:T(8,128)}, f32[256,2]{0,1:T(2,128)S(1)}, /*index=5*/f3...) while((s32[]{:T(128)}, f32[256,2]{0,1:T(2,128)S(1)}, ...), condition=%wide.region_5.6_spmd.clone, body=%wide.region_0.5_spmd.clone.sunk | while | flops 204870656 | bytes 9381043 | solution.py:96
  82.7 1.3 fusion.60
  84.2 1.3 fusion.62
  86.3 1.8 constant_dynamic-slice_fusion.2
  88.1 1.1 copy.33
  89.2 1.7 fusion.68
  90.9 1.0 fusion.67
  92.0 1.3 fusion.60
  93.4 1.3 fusion.62
  94.8 1.3 fusion.66
  96.2 1.8 constant_dynamic-slice_fusion.2
  98.0 1.1 copy.33
  99.1 2.0 fusion.68
  101.1 2.0 fusion.67
  103.1 1.3 fusion.60
  104.5 1.3 fusion.62
  106.0 1.3 fusion.66
  107.3 1.8 constant_dynamic-slice_fusion.2
  109.1 1.1 copy.33
  110.2 2.0 fusion.68
  112.2 2.0 fusion.67
  114.2 1.3 fusion.60
  115.6 1.3 fusion.62
  117.1 1.3 fusion.66
  118.4 1.8 constant_dynamic-slice_fusion.2
  120.2 1.1 copy.33
  121.4 2.0 fusion.68
  123.4 2.0 fusion.67
  125.3 1.2 multiply_reduce_fusion.1
  127.3 1.5 convolution_convert_fusion.1
  129.0 2.5 stack.2
  131.5 4.9 %all-to-all-start = ((bf16[8,1024,256]{1,2,0:T(8,128)(2,1)}), bf16[8,1024,256]{1,2,0:T(8,128)(2,1)}, u32[]{:S(2)}, u32[]{:S(2)}) async-start(bf16[8,1024,256]{1,2,0:T(8,128)(2,1)} %stack.2), calls=%async_computation | async-start | bytes 8388608 | tf_op jit(solution)/shard_map/all_to_all | solution.py:120
  137.1 28.8 %all-reduce.2.cloned.1.call-done = bf16[256,2048]{1,0:T(8,128)(2,1)} async-done(((bf16[256,2048]{1,0:T(8,128)(2,1)}), bf16[256,2048]{1,0:T(8,128)(2,1)}) %all-reduce.2.cloned.1.call-update) | async-done | bytes 1048592 | tf_op jit(solution)/shard_map/psum | solution.py:106
  165.9 2.0 fusion.25
  168.9 97.4 %all-to-all-done = bf16[8,1024,256]{1,2,0:T(8,128)(2,1)} async-done(((bf16[8,1024,256]{1,2,0:T(8,128)(2,1)}), bf16[8,1024,256]{1,2,0:T(8,128)(2,1)}, u32[]{:S(2)}, u32[]{:S(2)}) %all-to-all-start) | async-done | bytes 4194336 | tf_op jit(solution)/shard_map/all_to_all | solution.py:120
  266.3 3.2 %all-gather.8.cloned.1.call-done = bf16[2048,1024]{1,0:T(8,128)(2,1)} async-done(((bf16[256,1024]{1,0:T(8,128)(2,1)}), bf16[2048,1024]{1,0:T(8,128)(2,1)}) %all-gather.8.cloned.1.call-update) | async-done | bytes 4194320 | tf_op jit(solution)/shard_map/all_gather | solution.py:116
  269.6 6.9 %convolution_convert_fusion = bf16[256,2048]{1,0:T(8,128)(2,1)} fusion(bf16[1024,2048]{0,1:T(8,128)(2,1)} %bitcast.8, bf16[256,2048]{1,0:T(8,128)(2,1)S(1)} %multiply_convert_fusion, bf16[2048,1024]{1,0:T(8,128)(2,1)} %all-gather.8.cloned.1.call-done), kind=kOutput, calls=%fused_computation.37 | convolution fusion | flops 2148794368 | bytes 10485760 | tf_op jit(solution)/shard_map/dot_general | solution.py:124
  276.5 23.7 %reduce-scatter.2.cloned.1.call-done = bf16[64,2048]{1,0:T(8,128)(2,1)} async-done(((bf16[256,2048]{1,0:T(8,128)(2,1)}), bf16[64,2048]{1,0:T(8,128)(2,1)}) %reduce-scatter.2.cloned.1.call-update) | async-done | bytes 262160 | tf_op jit(solution)/shard_map/reduce_scatter | solution.py:123
  300.2 1.7 add_convert_fusion
  (77 shorter events, 7.2 us)
Async XLA Ops:
  6.5 120.8 %copy-start = (bf16[256,2048]{1,0:T(8,128)(2,1)S(1)}, bf16[256,2048]{1,0:T(8,128)(2,1)}, u32[]{:S(2)}) copy-start(bf16[256,2048]{1,0:T(8,128)(2,1)} %param.22) | copy-start | bytes 3145732
  6.5 74.1 %all-gather.6.cloned.1.call-start = ((), (), s32[]{:S(2)}) async-start(), calls=%async_computation.3 | async-start | bytes 1179648 | tf_op jit(solution)/shard_map/all_gather | solution.py:76
  7.3 129.8 %all-gather.4.cloned.1.call-start = ((), (), s32[]{:S(2)}) async-start(), calls=%async_computation.2 | async-start | bytes 1310720 | tf_op jit(solution)/shard_map/all_gather | solution.py:109
  8.0 157.9 %all-reduce.2.cloned.1.call-start = ((), (), s32[]{:S(2)}) async-start(), calls=%async_computation.4 | async-start | bytes 2097152 | tf_op jit(solution)/shard_map/psum | solution.py:106
  86.3 4.7 %copy-start.4 = (f32[256,2]{0,1:T(2,128)S(1)}, f32[256,2]{0,1:T(2,128)}, u32[]{:S(2)}) copy-start(f32[256,2]{0,1:T(2,128)} %get-tuple-element.265) | copy-start | bytes 6148 | tf_op jit(solution)/shard_map/while
  96.2 4.9 %copy-start.4 = (f32[256,2]{0,1:T(2,128)S(1)}, f32[256,2]{0,1:T(2,128)}, u32[]{:S(2)}) copy-start(f32[256,2]{0,1:T(2,128)} %get-tuple-element.265) | copy-start | bytes 6148 | tf_op jit(solution)/shard_map/while
  107.3 4.9 %copy-start.4 = (f32[256,2]{0,1:T(2,128)S(1)}, f32[256,2]{0,1:T(2,128)}, u32[]{:S(2)}) copy-start(f32[256,2]{0,1:T(2,128)} %get-tuple-element.265) | copy-start | bytes 6148 | tf_op jit(solution)/shard_map/while
  118.4 4.9 %copy-start.4 = (f32[256,2]{0,1:T(2,128)S(1)}, f32[256,2]{0,1:T(2,128)}, u32[]{:S(2)}) copy-start(f32[256,2]{0,1:T(2,128)} %get-tuple-element.265) | copy-start | bytes 6148 | tf_op jit(solution)/shard_map/while
  125.3 3.5 %copy-start.3 = (bf16[1024,256]{1,0:T(8,128)(2,1)S(1)}, bf16[1024,256]{1,0:T(8,128)(2,1)}, u32[]{:S(2)}) copy-start(bf16[1024,256]{1,0:T(8,128)(2,1)} %param.25) | copy-start | bytes 1572868
  131.5 134.8 %all-to-all-start = ((bf16[8,1024,256]{1,2,0:T(8,128)(2,1)}), bf16[8,1024,256]{1,2,0:T(8,128)(2,1)}, u32[]{:S(2)}, u32[]{:S(2)}) async-start(bf16[8,1024,256]{1,2,0:T(8,128)(2,1)} %stack.2), calls=%async_computation | async-start | bytes 8388608 | tf_op jit(solution)/shard_map/all_to_all | solution.py:120
  136.4 133.2 %all-gather.8.cloned.1.call-start = ((), (), s32[]{:S(2)}) async-start(), calls=%async_computation.5 | async-start | bytes 4718592 | tf_op jit(solution)/shard_map/all_gather | solution.py:116
  136.4 32.0 %copy-start.5 = (f32[2048]{0:T(1024)S(1)}, f32[2048]{0:T(1024)}, u32[]{:S(2)}) copy-start(f32[2048]{0:T(1024)} %param.23) | copy-start | bytes 24580
  137.0 163.2 %reduce-scatter.2.cloned.1.call-start = ((), (), s32[]{:S(2)}) async-start(), calls=%async_computation.6 | async-start | bytes 1310720 | tf_op jit(solution)/shard_map/reduce_scatter | solution.py:123
  137.0 30.8 %copy-start.1 = (bf16[256,2048]{1,0:T(8,128)(2,1)S(1)}, bf16[256,2048]{1,0:T(8,128)(2,1)}, u32[]{:S(2)}) copy-start(bf16[256,2048]{1,0:T(8,128)(2,1)} %all-gather.4.cloned.1.call-done) | copy-start | bytes 3145732
  165.9 2.0 copy-start.2
Sparse Core Ops, SparseCore 0:
  9.5 45.4 all-gather.5
  56.5 15.4 all-gather.3
  128.9 36.9 all-reduce.1
  167.9 101.6 all-gather.7
  276.6 23.5 reduce-scatter.1
